TPU v7x, 32 devices: a whole 2x2x4 slice. The times are simulated.
32 devices in a mesh: fs: 8 (over z, x), tp: 4 (over y, core).
Axes of the slice: x: 2, y: 2, z: 4, core: 2. Of those that a mesh axis runs over, the one named last changes fastest.
Arguments:
- prompt_rows: bfloat16 [512, 3072], P('tp'), may hold values from -6 to 6
- gate_first: float32 [3072, 8192], P('fs', 'tp'), may hold values from -0.109375 to 0.109375
- up_first: float32 [3072, 8192], P('fs', 'tp'), may hold values from -0.109375 to 0.109375
- down_first: float32 [8192, 3072], P('fs', 'tp'), may hold values from -0.0625 to 0.0625
- gate_second: float32 [3072, 8192], P('fs', 'tp'), may hold values from -0.109375 to 0.109375
- up_second: float32 [3072, 8192], P('fs', 'tp'), may hold values from -0.109375 to 0.109375
- down_second: float32 [8192, 3072], P('fs', 'tp'), may hold values from -0.0625 to 0.0625
- pre_gain_first: float32 [3072], replicated, may hold values from 0.1 to 1.9
- post_gain_first: float32 [3072], replicated, may hold values from 0.1 to 1.9
- pre_gain_second: float32 [3072], replicated, may hold values from 0.1 to 1.9
- post_gain_second: float32 [3072], replicated, may hold values from 0.1 to 1.9
Outputs:
- result_rows: bfloat16 [512, 3072], P('tp')
- gate_first_new: bfloat16 [3072, 8192], P(None, 'fs')
- up_first_new: bfloat16 [3072, 8192], P(None, 'fs')
- down_first_new: bfloat16 [8192, 3072], P('fs')
- gate_second_new: bfloat16 [3072, 8192], P(None, 'fs')
- up_second_new: bfloat16 [3072, 8192], P(None, 'fs')
- down_second_new: bfloat16 [8192, 3072], P('fs')
All inputs are finite; a program needn't handle non-finite values.
Results may differ from a plain program's by a relative error of at most 0.0071.
Values may be sent and summed in bfloat16 or wider, within the bound.
A program may use at most 192 MiB of HBM per device.

v0:
```python
import jax
import jax.numpy as jnp
from jax import lax
from jax.sharding import PartitionSpec as P

EPSILON = 1e-06


def half_step(rows, gate, up, down, post_gain):
    floats = rows.astype(jnp.float32)
    normed = (
        floats * lax.rsqrt(jnp.mean(floats * floats, axis=-1, keepdims=True) + EPSILON)
    ).astype(jnp.bfloat16)
    gate_pre = jnp.dot(normed, gate, preferred_element_type=jnp.float32)
    up_pre = jnp.dot(normed, up, preferred_element_type=jnp.float32)
    hidden = (jax.nn.silu(gate_pre) * up_pre).astype(jnp.bfloat16)
    partial_value = jnp.dot(hidden, down, preferred_element_type=jnp.float32)
    total = lax.psum(partial_value, "fs")
    scale = lax.rsqrt(jnp.mean(total * total, axis=-1, keepdims=True) + EPSILON)
    return (floats + 0.5 * total * scale * post_gain[None, :]).astype(jnp.bfloat16)


def per_device(
    prompt_rows,
    gate_first,
    up_first,
    down_first,
    gate_second,
    up_second,
    down_second,
    pre_gain_first,
    post_gain_first,
    pre_gain_second,
    post_gain_second,
):
    height = gate_first.shape[0]
    start = lax.axis_index("fs") * height
    gain_a = lax.dynamic_slice_in_dim(pre_gain_first, start, height, 0)[:, None]
    gain_b = lax.dynamic_slice_in_dim(pre_gain_second, start, height, 0)[:, None]
    wide = (
        lax.all_gather((gain_a * gate_first).astype(jnp.bfloat16), "tp", axis=1, tiled=True),
        lax.all_gather((gain_a * up_first).astype(jnp.bfloat16), "tp", axis=1, tiled=True),
        lax.all_gather(down_first.astype(jnp.bfloat16), "tp", axis=1, tiled=True),
        lax.all_gather((gain_b * gate_second).astype(jnp.bfloat16), "tp", axis=1, tiled=True),
        lax.all_gather((gain_b * up_second).astype(jnp.bfloat16), "tp", axis=1, tiled=True),
        lax.all_gather(down_second.astype(jnp.bfloat16), "tp", axis=1, tiled=True),
    )
    gate_a, up_a, gate_b, up_b = (
        lax.all_to_all(wide[0], "fs", split_axis=1, concat_axis=0, tiled=True),
        lax.all_to_all(wide[1], "fs", split_axis=1, concat_axis=0, tiled=True),
        lax.all_to_all(wide[3], "fs", split_axis=1, concat_axis=0, tiled=True),
        lax.all_to_all(wide[4], "fs", split_axis=1, concat_axis=0, tiled=True),
    )
    down_a = wide[2]
    down_b = wide[5]
    middle = half_step(prompt_rows, gate_a, up_a, down_a, post_gain_first)
    result = half_step(middle, gate_b, up_b, down_b, post_gain_second)
    return (result, gate_a, up_a, down_a, gate_b, up_b, down_b)


def solution(mesh):
    return jax.shard_map(
        per_device,
        mesh=mesh,
        in_specs=(
            P("tp", None),
            P("fs", "tp"),
            P("fs", "tp"),
            P("fs", "tp"),
            P("fs", "tp"),
            P("fs", "tp"),
            P("fs", "tp"),
            P(),
            P(),
            P(),
            P(),
        ),
        out_specs=(
            P("tp", None),
            P(None, "fs"),
            P(None, "fs"),
            P("fs", None),
            P(None, "fs"),
            P(None, "fs"),
            P("fs", None),
        ),
        check_vma=False,
    )
```

profile of v0, /device:TPU:0, one launch (start us, length us, event | category | flops | bytes accessed | tf_op | source)
XLA Modules:
  0.0 843.3 jit_solution(3647729259422297711)
XLA Ops:
  7.2 0.0 all-gather.7.cloned.1.call-start
  7.2 0.8 dynamic_slice.6
  8.0 5.5 multiply_convert_fusion.3
  13.5 0.0 all-gather.7.cloned.1.call-update
  13.5 0.0 all-gather.9.cloned.1.call-start
  13.6 0.7 all-gather.9.cloned.1.call-update
  14.3 48.5 %all-gather.7.cloned.1.call-done = bf16[384,8192]{1,0:T(8,128)(2,1)} async-done(((bf16[384,2048]{1,0:T(8,128)(2,1)}), bf16[384,8192]{1,0:T(8,128)(2,1)}) %all-gather.7.cloned.1.call-update) | async-done | bytes 6291472 | tf_op jit(solution)/shard_map/all_gather | solution.py:41
  62.7 6.5 copy.33
  69.2 5.8 all-to-all-start
  75.0 0.0 all-gather.13.cloned.1.call-start
  75.1 0.8 dynamic_slice.7
  75.8 0.0 copy-done.1
  75.8 4.5 multiply_convert_fusion.1
  80.4 0.0 all-gather.13.cloned.1.call-update
  80.4 30.9 %all-gather.9.cloned.1.call-done = bf16[384,8192]{1,0:T(8,128)(2,1)} async-done(((bf16[384,2048]{1,0:T(8,128)(2,1)}), bf16[384,8192]{1,0:T(8,128)(2,1)}) %all-gather.9.cloned.1.call-update) | async-done | bytes 6291472 | tf_op jit(solution)/shard_map/all_gather | solution.py:42
  111.3 6.5 copy.32
  117.8 95.9 %all-to-all-done = bf16[384,8,1024]{2,0,1:T(8,128)(2,1)} async-done(((bf16[384,8,1024]{2,0,1:T(8,128)(2,1)}), bf16[384,8,1024]{2,0,1:T(8,128)(2,1)}, u32[]{:S(2)}, u32[]{:S(2)}) %all-to-all-start) | async-done | bytes 6291488 | tf_op jit(solution)/shard_map/all_to_all | solution.py:49
  213.7 4.8 all-to-all-start.1
  218.4 0.0 all-gather.15.cloned.1.call-start
  218.5 0.5 all-gather.15.cloned.1.call-update
  219.0 0.0 all-gather.13.cloned.1.call-done
  219.0 6.5 copy.31
  225.5 130.6 %all-to-all-done.1 = bf16[384,8,1024]{2,0,1:T(8,128)(2,1)} async-done(((bf16[384,8,1024]{2,0,1:T(8,128)(2,1)}), bf16[384,8,1024]{2,0,1:T(8,128)(2,1)}, u32[]{:S(2)}, u32[]{:S(2)}) %all-to-all-start.1) | async-done | bytes 6291488 | tf_op jit(solution)/shard_map/all_to_all | solution.py:50
  356.1 4.8 all-to-all-start.2
  361.0 0.0 copy-start
  361.0 0.0 all-gather.11.cloned.1.call-start
  361.0 3.2 convert_element_type.47
  364.3 0.0 all-gather.11.cloned.1.call-update
  364.3 0.0 all-reduce.3.cloned.1.call-start
  364.3 0.0 copy-done
  364.4 0.2 fusion
  364.6 0.0 all-gather.15.cloned.1.call-done
  364.6 6.5 copy.30
  371.1 4.6 fusion.26
  375.7 35.5 %all-gather.11.cloned.1.call-done = bf16[1024,3072]{1,0:T(8,128)(2,1)} async-done(((bf16[1024,768]{1,0:T(8,128)(2,1)}), bf16[1024,3072]{1,0:T(8,128)(2,1)}) %all-gather.11.cloned.1.call-update) | async-done | bytes 6291472 | tf_op jit(solution)/shard_map/all_gather | solution.py:43
  411.2 7.7 fusion.9
  418.9 0.0 all-reduce.3.cloned.1.call-update
  418.9 100.4 %all-to-all-done.2 = bf16[384,8,1024]{2,0,1:T(8,128)(2,1)} async-done(((bf16[384,8,1024]{2,0,1:T(8,128)(2,1)}), bf16[384,8,1024]{2,0,1:T(8,128)(2,1)}, u32[]{:S(2)}, u32[]{:S(2)}) %all-to-all-start.2) | async-done | bytes 6291488 | tf_op jit(solution)/shard_map/all_to_all | solution.py:51
  519.3 4.8 all-to-all-start.3
  524.1 0.0 copy-start.2
  524.1 0.0 all-gather.17.cloned.1.call-start
  524.2 3.3 convert_element_type.54
  527.4 0.0 all-gather.17.cloned.1.call-update
  527.4 0.2 all-reduce.5.cloned.1.call-start
  527.7 130.8 %all-reduce.3.cloned.1.call-done = f32[128,3072]{1,0:T(8,128)} async-done(((f32[128,3072]{1,0:T(8,128)}), f32[128,3072]{1,0:T(8,128)}) %all-reduce.3.cloned.1.call-update) | async-done | bytes 1572880 | tf_op jit(solution)/shard_map/psum | solution.py:18
  658.5 1.6 multiply_reduce_fusion.1
  660.1 0.0 copy-done.2
  660.1 1.9 fusion.3
  662.0 4.2 fusion.22
  666.3 38.0 %all-gather.17.cloned.1.call-done = bf16[1024,3072]{1,0:T(8,128)(2,1)} async-done(((bf16[1024,768]{1,0:T(8,128)(2,1)}), bf16[1024,3072]{1,0:T(8,128)(2,1)}) %all-gather.17.cloned.1.call-update) | async-done | bytes 6291472 | tf_op jit(solution)/shard_map/all_gather | solution.py:46
  704.2 0.0 all-to-all-done.3
  704.2 7.7 fusion.8
  711.9 0.0 all-reduce.5.cloned.1.call-update
  712.0 89.4 %all-reduce.5.cloned.1.call-done = f32[128,3072]{1,0:T(8,128)} async-done(((f32[128,3072]{1,0:T(8,128)}), f32[128,3072]{1,0:T(8,128)}) %all-reduce.5.cloned.1.call-update) | async-done | bytes 1572880 | tf_op jit(solution)/shard_map/psum | solution.py:18
  801.4 1.6 multiply_reduce_fusion
  803.0 0.0 copy-done.3
  803.0 2.6 fusion.5
  805.6 6.4 copy.42
  812.0 6.3 copy.43
  818.3 2.7 copy.44
  821.0 6.4 copy.45
  827.4 6.3 copy.46
  833.8 0.0 slice-done.2
  833.8 2.7 copy.47
  (15 shorter events, 0.1 us)
Async XLA Ops:
  7.2 55.6 %all-gather.7.cloned.1.call-start = ((), (), s32[]{:S(2)}) async-start(), calls=%async_computation.4 | async-start | bytes 7864320 | tf_op jit(solution)/shard_map/all_gather | solution.py:41
  13.5 97.8 %all-gather.9.cloned.1.call-start = ((), (), s32[]{:S(2)}) async-start(), calls=%async_computation.5 | async-start | bytes 7864320 | tf_op jit(solution)/shard_map/all_gather | solution.py:42
  69.2 6.6 copy-start.1
  69.2 144.4 %all-to-all-start = ((bf16[384,8,1024]{2,0,1:T(8,128)(2,1)}), bf16[384,8,1024]{2,0,1:T(8,128)(2,1)}, u32[]{:S(2)}, u32[]{:S(2)}) async-start(bf16[384,8,1024]{2,0,1:T(8,128)(2,1)} %bitcast.40), calls=%async_computation | async-start | bytes 12582912 | tf_op jit(solution)/shard_map/all_to_all | solution.py:49
  75.0 144.0 %all-gather.13.cloned.1.call-start = ((), (), s32[]{:S(2)}) async-start(), calls=%async_computation.8 | async-start | bytes 7864320 | tf_op jit(solution)/shard_map/all_gather | solution.py:44
  213.7 142.5 %all-to-all-start.1 = ((bf16[384,8,1024]{2,0,1:T(8,128)(2,1)}), bf16[384,8,1024]{2,0,1:T(8,128)(2,1)}, u32[]{:S(2)}, u32[]{:S(2)}) async-start(bf16[384,8,1024]{2,0,1:T(8,128)(2,1)} %bitcast.41), calls=%async_computation.1 | async-start | bytes 12582912 | tf_op jit(solution)/shard_map/all_to_all | solution.py:50
  218.4 146.2 %all-gather.15.cloned.1.call-start = ((), (), s32[]{:S(2)}) async-start(), calls=%async_computation.9 | async-start | bytes 7864320 | tf_op jit(solution)/shard_map/all_gather | solution.py:45
  356.1 163.1 %all-to-all-start.2 = ((bf16[384,8,1024]{2,0,1:T(8,128)(2,1)}), bf16[384,8,1024]{2,0,1:T(8,128)(2,1)}, u32[]{:S(2)}, u32[]{:S(2)}) async-start(bf16[384,8,1024]{2,0,1:T(8,128)(2,1)} %bitcast.39), calls=%async_computation.2 | async-start | bytes 12582912 | tf_op jit(solution)/shard_map/all_to_all | solution.py:51
  361.0 3.4 copy-start
  361.0 50.2 %all-gather.11.cloned.1.call-start = ((), (), s32[]{:S(2)}) async-start(), calls=%async_computation.6 | async-start | bytes 7864320 | tf_op jit(solution)/shard_map/all_gather | solution.py:43
  364.3 294.2 %all-reduce.3.cloned.1.call-start = ((), (), s32[]{:S(2)}) async-start(), calls=%async_computation.7 | async-start | bytes 3145728 | tf_op jit(solution)/shard_map/psum | solution.py:18
  519.3 185.0 %all-to-all-start.3 = ((bf16[384,8,1024]{2,0,1:T(8,128)(2,1)}), bf16[384,8,1024]{2,0,1:T(8,128)(2,1)}, u32[]{:S(2)}, u32[]{:S(2)}) async-start(bf16[384,8,1024]{2,0,1:T(8,128)(2,1)} %bitcast.38), calls=%async_computation.3 | async-start | bytes 12582912 | tf_op jit(solution)/shard_map/all_to_all | solution.py:52
  524.1 136.0 %copy-start.2 = (f32[3072]{0:T(1024)S(1)}, f32[3072]{0:T(1024)}, u32[]{:S(2)}) copy-start(f32[3072]{0:T(1024)} %param.19) | copy-start | bytes 36868
  524.1 180.1 %all-gather.17.cloned.1.call-start = ((), (), s32[]{:S(2)}) async-start(), calls=%async_computation.10 | async-start | bytes 7864320 | tf_op jit(solution)/shard_map/all_gather | solution.py:46
  527.4 273.9 %all-reduce.5.cloned.1.call-start = ((), (), s32[]{:S(2)}) async-start(), calls=%async_computation.11 | async-start | bytes 3145728 | tf_op jit(solution)/shard_map/psum | solution.py:18
  711.9 91.1 %copy-start.3 = (f32[3072]{0:T(1024)S(1)}, f32[3072]{0:T(1024)}, u32[]{:S(2)}) copy-start(f32[3072]{0:T(1024)} %param.21) | copy-start | bytes 36868
  805.6 12.7 %slice-start = ((s8[6291456]{0:T(1024)(128)(4,1)}), s8[4194304]{0:T(1024)(128)(4,1)S(1)}, s32[]{:S(2)}) async-start(s8[6291456]{0:T(1024)(128)(4,1)} %bitcast.34), calls=%async_computation.12 | async-start | bytes 8388608
  812.0 6.4 slice-start.1
  821.0 12.7 %slice-start.2 = ((s8[6291456]{0:T(1024)(128)(4,1)}), s8[4194304]{0:T(1024)(128)(4,1)S(1)}, s32[]{:S(2)}) async-start(s8[6291456]{0:T(1024)(128)(4,1)} %bitcast.36), calls=%async_computation.14 | async-start | bytes 8388608
  827.4 6.4 slice-start.3
Sparse Core Ops, SparseCore 0:
  13.6 49.0 all-gather.6
  64.9 46.3 all-gather.8
  113.4 46.3 all-gather.12
  221.1 46.7 all-gather.14
  364.4 46.6 all-gather.10
  419.0 239.4 all-reduce.2
  660.6 43.5 all-gather.16
  712.1 89.2 all-reduce.4
where the time goes:
time: 844 us; the launch traced here: 843 us
  waiting for transfers between devices  701 us (83%)
  local copies, waits for them, and re-layouts  58.5 us (7%)
  other arithmetic  24.5 us (3%)
  matrix products  24.2 us (3%)
  starting transfers between devices  20.7 us (2%)
  between operations  14.3 us (2%)
    psum x2, waiting for transfers between devices, half_step(): total = lax.psum(partial_value, 'fs')  220 us
    all_to_all x1, waiting for transfers between devices, per_device(): lax.all_to_all(wide[1], 'fs', split_axis=1, concat_axis=0, tiled=True)  131 us
    all_to_all x1, waiting for transfers between devices, per_device(): lax.all_to_all(wide[3], 'fs', split_axis=1, concat_axis=0, tiled=True)  100 us
    all_to_all x1, waiting for transfers between devices, per_device(): lax.all_to_all(wide[0], 'fs', split_axis=1, concat_axis=0, tiled=True)  95.9 us
    all_gather x1, waiting for transfers between devices, per_device(): lax.all_gather((gain_a * gate_first).astype(jnp.bfloat16), 'tp', axis=1,...  48.5 us
    all_gather x1, waiting for transfers between devices, per_device(): lax.all_gather(down_second.astype(jnp.bfloat16), 'tp', axis=1, tiled=True)  38 us
    all_gather x1, waiting for transfers between devices, per_device(): lax.all_gather(down_first.astype(jnp.bfloat16), 'tp', axis=1, tiled=True)  35.5 us
    unnamed x22, local copies, waits for them, and re-layouts  30.9 us
  transfers between devices with their start and end apart: 12, of which 9 were waited for; matrix products, arithmetic and copies ran while one was open for 7% of the time, Pallas kernels for 0%

commit v1 on v0

--- a/solution.py
+++ b/solution.py
@@ -15,7 +15,9 @@
     up_pre = jnp.dot(normed, up, preferred_element_type=jnp.float32)
     hidden = (jax.nn.silu(gate_pre) * up_pre).astype(jnp.bfloat16)
     partial_value = jnp.dot(hidden, down, preferred_element_type=jnp.float32)
-    total = lax.psum(partial_value, "fs")
+    total = partial_value
+    for hop in (1, 2, 4):
+        total = total + lax.ppermute(total, "fs", [(dev, dev ^ hop) for dev in range(8)])
     scale = lax.rsqrt(jnp.mean(total * total, axis=-1, keepdims=True) + EPSILON)
     return (floats + 0.5 * total * scale * post_gain[None, :]).astype(jnp.bfloat16)
 

time: 844 us -> 936 us (1.11)
  waiting for transfers between devices: 701 us -> 793 us
  starting transfers between devices: 20.7 us -> 30.5 us
    ppermute x0 -> x6, waiting for transfers between devices: none -> 357 us  [half_step(): lax.ppermute(total, 'fs', [(dev, dev ^ hop) for dev in range(8)])]
    psum x2 -> x0, waiting for transfers between devices: 220 us -> none  [half_step(): total = lax.psum(partial_value, 'fs')]
    all_gather x1, waiting for transfers between devices: 38 us -> 0.02 us  [per_device(): lax.all_gather(down_second.astype(jnp.bfloat16), 'tp', axis=1, tiled=True)]
    all_gather x1, waiting for transfers between devices: 35.5 us -> 0.02 us  [per_device(): lax.all_gather(down_first.astype(jnp.bfloat16), 'tp', axis=1, tiled=True)]
    all_to_all x1, waiting for transfers between devices: 100 us -> 129 us  [per_device(): lax.all_to_all(wide[3], 'fs', split_axis=1, concat_axis=0, tiled=True)]
    ppermute x0 -> x6, starting transfers between devices: none -> 9.54 us  [half_step(): lax.ppermute(total, 'fs', [(dev, dev ^ hop) for dev in range(8)])]
    unnamed x22 -> x26, local copies, waits for them, and re-layouts: 30.9 us -> 32 us
  transfers between devices with their start and end apart: 12 -> 16, of which waited for: 9 -> 11; matrix products, arithmetic and copies ran while one was open for 7% -> 5% of each run, Pallas kernels for 0% -> 0%
where the time goes in v1:
time: 936 us
  waiting for transfers between devices  793 us (85%)
  local copies, waits for them, and re-layouts  59.6 us (6%)
  starting transfers between devices  30.5 us (3%)
  matrix products  21.9 us (2%)
  other arithmetic  16 us (2%)
  between operations  14.3 us (2%)
    ppermute x6, waiting for transfers between devices, half_step(): lax.ppermute(total, 'fs', [(dev, dev ^ hop) for dev in range(8)])  357 us
    all_to_all x1, waiting for transfers between devices, per_device(): lax.all_to_all(wide[1], 'fs', split_axis=1, concat_axis=0, tiled=True)  131 us
    all_to_all x1, waiting for transfers between devices, per_device(): lax.all_to_all(wide[3], 'fs', split_axis=1, concat_axis=0, tiled=True)  129 us
    all_to_all x1, waiting for transfers between devices, per_device(): lax.all_to_all(wide[0], 'fs', split_axis=1, concat_axis=0, tiled=True)  95.9 us
    all_gather x1, waiting for transfers between devices, per_device(): lax.all_gather((gain_a * gate_first).astype(jnp.bfloat16), 'tp', axis=1,...  48.5 us
    unnamed x26, local copies, waits for them, and re-layouts  32 us
    all_gather x1, waiting for transfers between devices, per_device(): lax.all_gather((gain_a * up_first).astype(jnp.bfloat16), 'tp', axis=1, ti...  30.9 us
  transfers between devices with their start and end apart: 16, of which 11 were waited for; matrix products, arithmetic and copies ran while one was open for 5% of the time, Pallas kernels for 0%

profile of v1, /device:TPU:0, one launch (start us, length us, event | category | flops | bytes accessed | tf_op | source)
XLA Modules:
  0.0 935.5 jit_solution(4626363899245537802)
XLA Ops:
  7.2 0.0 all-gather.7.cloned.1.call-start
  7.2 0.8 dynamic_slice.6
  8.0 5.5 multiply_convert_fusion.3
  13.5 0.0 all-gather.9.cloned.1.call-start
  13.6 0.7 all-gather.9.cloned.1.call-update
  14.3 48.5 %all-gather.7.cloned.1.call-done = bf16[384,8192]{1,0:T(8,128)(2,1)} async-done(((bf16[384,2048]{1,0:T(8,128)(2,1)}), bf16[384,8192]{1,0:T(8,128)(2,1)}) %all-gather.7.cloned.1.call-update) | async-done | bytes 6291472 | tf_op jit(solution)/shard_map/all_gather | solution.py:43
  62.7 6.5 copy.33
  69.2 5.8 all-to-all-start
  75.0 0.0 all-gather.13.cloned.1.call-start
  75.1 0.8 dynamic_slice.7
  75.8 4.5 multiply_convert_fusion
  80.4 0.0 all-gather.13.cloned.1.call-update
  80.4 30.9 %all-gather.9.cloned.1.call-done = bf16[384,8192]{1,0:T(8,128)(2,1)} async-done(((bf16[384,2048]{1,0:T(8,128)(2,1)}), bf16[384,8192]{1,0:T(8,128)(2,1)}) %all-gather.9.cloned.1.call-update) | async-done | bytes 6291472 | tf_op jit(solution)/shard_map/all_gather | solution.py:44
  111.3 6.5 copy.32
  117.8 95.9 %all-to-all-done = bf16[384,8,1024]{2,0,1:T(8,128)(2,1)} async-done(((bf16[384,8,1024]{2,0,1:T(8,128)(2,1)}), bf16[384,8,1024]{2,0,1:T(8,128)(2,1)}, u32[]{:S(2)}, u32[]{:S(2)}) %all-to-all-start) | async-done | bytes 6291488 | tf_op jit(solution)/shard_map/all_to_all | solution.py:51
  213.7 4.7 all-to-all-start.1
  218.4 0.0 all-gather.15.cloned.1.call-start
  218.4 0.5 all-gather.15.cloned.1.call-update
  219.0 0.0 all-gather.13.cloned.1.call-done
  219.0 6.5 copy.31
  225.5 130.6 %all-to-all-done.1 = bf16[384,8,1024]{2,0,1:T(8,128)(2,1)} async-done(((bf16[384,8,1024]{2,0,1:T(8,128)(2,1)}), bf16[384,8,1024]{2,0,1:T(8,128)(2,1)}, u32[]{:S(2)}, u32[]{:S(2)}) %all-to-all-start.1) | async-done | bytes 6291488 | tf_op jit(solution)/shard_map/all_to_all | solution.py:52
  356.1 5.0 all-to-all-start.2
  361.1 0.0 all-gather.11.cloned.1.call-start
  361.2 1.3 convert_element_type.47
  362.5 0.0 all-gather.15.cloned.1.call-done
  362.6 6.5 copy.30
  369.1 129.3 %all-to-all-done.2 = bf16[384,8,1024]{2,0,1:T(8,128)(2,1)} async-done(((bf16[384,8,1024]{2,0,1:T(8,128)(2,1)}), bf16[384,8,1024]{2,0,1:T(8,128)(2,1)}, u32[]{:S(2)}, u32[]{:S(2)}) %all-to-all-start.2) | async-done | bytes 6291488 | tf_op jit(solution)/shard_map/all_to_all | solution.py:53
  498.4 5.0 all-to-all-start.3
  503.4 0.2 all-gather.17.cloned.1.call-start
  503.7 1.3 convert_element_type.54
  505.0 1.1 copy-done
  506.1 0.2 fusion
  506.3 3.8 fusion.24
  510.2 0.0 all-gather.11.cloned.1.call-done
  510.2 7.6 fusion.7
  517.9 1.6 collective-permute-start
  519.4 86.6 %collective-permute-done = f32[128,3072]{1,0:T(8,128)S(1)} collective-permute-done((f32[128,3072]{1,0:T(8,128)S(1)}, f32[128,3072]{1,0:T(8,128)S(1)}, u32[]{:S(2)}, u32[]{:S(2)}) %collective-permute-start) | collective-permute-done | bytes 1572896 | tf_op jit(solution)/shard_map/ppermute | solution.py:20
  606.0 0.2 add.70
  606.3 0.1 collective-permute-start.1
  606.4 66.6 %collective-permute-done.1 = f32[128,3072]{1,0:T(8,128)S(1)} collective-permute-done((f32[128,3072]{1,0:T(8,128)S(1)}, f32[128,3072]{1,0:T(8,128)S(1)}, u32[]{:S(2)}, u32[]{:S(2)}) %collective-permute-start.1) | collective-permute-done | bytes 1572896 | tf_op jit(solution)/shard_map/ppermute | solution.py:20
  673.0 0.2 add.71
  673.2 1.8 collective-permute-start.2
  675.0 68.3 %collective-permute-done.2 = f32[128,3072]{1,0:T(8,128)S(1)} collective-permute-done((f32[128,3072]{1,0:T(8,128)S(1)}, f32[128,3072]{1,0:T(8,128)S(1)}, u32[]{:S(2)}, u32[]{:S(2)}) %collective-permute-start.2) | collective-permute-done | bytes 1572896 | tf_op jit(solution)/shard_map/ppermute | solution.py:20
  743.3 0.3 multiply_reduce_fusion.1
  743.6 0.5 fusion.3
  744.1 3.8 fusion.15
  748.0 0.0 all-gather.17.cloned.1.call-done
  748.0 6.7 fusion.20
  754.7 0.1 collective-permute-start.3
  754.7 34.6 %collective-permute-done.3 = f32[128,3072]{1,0:T(8,128)S(1)} collective-permute-done((f32[128,3072]{1,0:T(8,128)S(1)}, f32[128,3072]{1,0:T(8,128)S(1)}, u32[]{:S(2)}, u32[]{:S(2)}) %collective-permute-start.3) | collective-permute-done | bytes 1572896 | tf_op jit(solution)/shard_map/ppermute | solution.py:20
  789.3 0.2 add.77
  789.6 2.5 collective-permute-start.4
  792.1 33.7 %collective-permute-done.4 = f32[128,3072]{1,0:T(8,128)S(1)} collective-permute-done((f32[128,3072]{1,0:T(8,128)S(1)}, f32[128,3072]{1,0:T(8,128)S(1)}, u32[]{:S(2)}, u32[]{:S(2)}) %collective-permute-start.4) | collective-permute-done | bytes 1572896 | tf_op jit(solution)/shard_map/ppermute | solution.py:20
  825.8 0.2 add.78
  826.0 3.4 collective-permute-start.5
  829.4 66.8 %collective-permute-done.5 = f32[128,3072]{1,0:T(8,128)S(1)} collective-permute-done((f32[128,3072]{1,0:T(8,128)S(1)}, f32[128,3072]{1,0:T(8,128)S(1)}, u32[]{:S(2)}, u32[]{:S(2)}) %collective-permute-start.5) | collective-permute-done | bytes 1572896 | tf_op jit(solution)/shard_map/ppermute | solution.py:20
  896.3 0.3 multiply_reduce_fusion
  896.6 1.2 fusion.5
  897.8 6.4 copy.40
  904.2 6.3 copy.41
  910.6 2.7 copy.42
  913.3 6.4 copy.43
  919.6 6.3 copy.44
  926.0 2.7 copy.45
  (29 shorter events, 0.1 us)
Async XLA Ops:
  7.2 55.6 %all-gather.7.cloned.1.call-start = ((), (), s32[]{:S(2)}) async-start(), calls=%async_computation.4 | async-start | bytes 7864320 | tf_op jit(solution)/shard_map/all_gather | solution.py:43
  13.5 97.8 %all-gather.9.cloned.1.call-start = ((), (), s32[]{:S(2)}) async-start(), calls=%async_computation.5 | async-start | bytes 7864320 | tf_op jit(solution)/shard_map/all_gather | solution.py:44
  69.2 6.6 copy-start.1
  69.2 144.4 %all-to-all-start = ((bf16[384,8,1024]{2,0,1:T(8,128)(2,1)}), bf16[384,8,1024]{2,0,1:T(8,128)(2,1)}, u32[]{:S(2)}, u32[]{:S(2)}) async-start(bf16[384,8,1024]{2,0,1:T(8,128)(2,1)} %bitcast.39), calls=%async_computation | async-start | bytes 12582912 | tf_op jit(solution)/shard_map/all_to_all | solution.py:51
  75.0 144.0 %all-gather.13.cloned.1.call-start = ((), (), s32[]{:S(2)}) async-start(), calls=%async_computation.7 | async-start | bytes 7864320 | tf_op jit(solution)/shard_map/all_gather | solution.py:46
  213.7 142.5 %all-to-all-start.1 = ((bf16[384,8,1024]{2,0,1:T(8,128)(2,1)}), bf16[384,8,1024]{2,0,1:T(8,128)(2,1)}, u32[]{:S(2)}, u32[]{:S(2)}) async-start(bf16[384,8,1024]{2,0,1:T(8,128)(2,1)} %bitcast.40), calls=%async_computation.1 | async-start | bytes 12582912 | tf_op jit(solution)/shard_map/all_to_all | solution.py:52
  218.4 144.2 %all-gather.15.cloned.1.call-start = ((), (), s32[]{:S(2)}) async-start(), calls=%async_computation.8 | async-start | bytes 7864320 | tf_op jit(solution)/shard_map/all_gather | solution.py:47
  356.1 5.1 copy-start.2
  356.1 142.3 %all-to-all-start.2 = ((bf16[384,8,1024]{2,0,1:T(8,128)(2,1)}), bf16[384,8,1024]{2,0,1:T(8,128)(2,1)}, u32[]{:S(2)}, u32[]{:S(2)}) async-start(bf16[384,8,1024]{2,0,1:T(8,128)(2,1)} %bitcast.41), calls=%async_computation.2 | async-start | bytes 12582912 | tf_op jit(solution)/shard_map/all_to_all | solution.py:53
  361.1 149.0 %all-gather.11.cloned.1.call-start = ((), (), s32[]{:S(2)}) async-start(), calls=%async_computation.6 | async-start | bytes 7864320 | tf_op jit(solution)/shard_map/all_gather | solution.py:45
  498.4 5.3 copy-start.3
  498.4 249.6 %all-to-all-start.3 = ((bf16[384,8,1024]{2,0,1:T(8,128)(2,1)}), bf16[384,8,1024]{2,0,1:T(8,128)(2,1)}, u32[]{:S(2)}, u32[]{:S(2)}) async-start(bf16[384,8,1024]{2,0,1:T(8,128)(2,1)} %bitcast.38), calls=%async_computation.3 | async-start | bytes 12582912 | tf_op jit(solution)/shard_map/all_to_all | solution.py:54
  503.4 244.6 %all-gather.17.cloned.1.call-start = ((), (), s32[]{:S(2)}) async-start(), calls=%async_computation.9 | async-start | bytes 7864320 | tf_op jit(solution)/shard_map/all_gather | solution.py:48
  505.0 1.1 copy-start
  517.9 88.2 %collective-permute-start = (f32[128,3072]{1,0:T(8,128)S(1)}, f32[128,3072]{1,0:T(8,128)S(1)}, u32[]{:S(2)}, u32[]{:S(2)}) collective-permute-start(f32[128,3072]{1,0:T(8,128)S(1)} %fusion.7), channel_id=1, source_target_pairs={{0,4},{4,0},{8,12},{12,8},{16,20},{20,16},{24,28},{28,24},{1,5},{5... | collective-permute-start | bytes 4718600 | tf_op jit(solution)/shard_map/ppermute | solution.py:20
  606.3 66.7 %collective-permute-start.1 = (f32[128,3072]{1,0:T(8,128)S(1)}, f32[128,3072]{1,0:T(8,128)S(1)}, u32[]{:S(2)}, u32[]{:S(2)}) collective-permute-start(f32[128,3072]{1,0:T(8,128)S(1)} %add.70), channel_id=1, source_target_pairs={{0,8},{4,12},{8,0},{12,4},{16,24},{20,28},{24,16},{28,20},{1,9},{5... | collective-permute-start | bytes 4718600 | tf_op jit(solution)/shard_map/ppermute | solution.py:20
  673.2 70.5 %copy-start.4 = (f32[3072]{0:T(1024)S(1)}, f32[3072]{0:T(1024)}, u32[]{:S(2)}) copy-start(f32[3072]{0:T(1024)} %param.19) | copy-start | bytes 36868
  673.2 70.1 %collective-permute-start.2 = (f32[128,3072]{1,0:T(8,128)S(1)}, f32[128,3072]{1,0:T(8,128)S(1)}, u32[]{:S(2)}, u32[]{:S(2)}) collective-permute-start(f32[128,3072]{1,0:T(8,128)S(1)} %add.71), channel_id=1, source_target_pairs={{0,16},{4,20},{8,24},{12,28},{16,0},{20,4},{24,8},{28,12},{1,17},{... | collective-permute-start | bytes 4718600 | tf_op jit(solution)/shard_map/ppermute | solution.py:20
  754.7 34.7 %collective-permute-start.3 = (f32[128,3072]{1,0:T(8,128)S(1)}, f32[128,3072]{1,0:T(8,128)S(1)}, u32[]{:S(2)}, u32[]{:S(2)}) collective-permute-start(f32[128,3072]{1,0:T(8,128)S(1)} %fusion.20), channel_id=1, source_target_pairs={{0,4},{4,0},{8,12},{12,8},{16,20},{20,16},{24,28},{28,24},{1,5},{5... | collective-permute-start | bytes 4718600 | tf_op jit(solution)/shard_map/ppermute | solution.py:20
  789.6 36.2 %collective-permute-start.4 = (f32[128,3072]{1,0:T(8,128)S(1)}, f32[128,3072]{1,0:T(8,128)S(1)}, u32[]{:S(2)}, u32[]{:S(2)}) collective-permute-start(f32[128,3072]{1,0:T(8,128)S(1)} %add.77), channel_id=1, source_target_pairs={{0,8},{4,12},{8,0},{12,4},{16,24},{20,28},{24,16},{28,20},{1,9},{5... | collective-permute-start | bytes 4718600 | tf_op jit(solution)/shard_map/ppermute | solution.py:20
  826.0 70.6 %copy-start.5 = (f32[3072]{0:T(1024)S(1)}, f32[3072]{0:T(1024)}, u32[]{:S(2)}) copy-start(f32[3072]{0:T(1024)} %param.21) | copy-start | bytes 36868
  826.0 70.3 %collective-permute-start.5 = (f32[128,3072]{1,0:T(8,128)S(1)}, f32[128,3072]{1,0:T(8,128)S(1)}, u32[]{:S(2)}, u32[]{:S(2)}) collective-permute-start(f32[128,3072]{1,0:T(8,128)S(1)} %add.78), channel_id=1, source_target_pairs={{0,16},{4,20},{8,24},{12,28},{16,0},{20,4},{24,8},{28,12},{1,17},{... | collective-permute-start | bytes 4718600 | tf_op jit(solution)/shard_map/ppermute | solution.py:20
  897.8 12.7 %slice-start = ((s8[6291456]{0:T(1024)(128)(4,1)}), s8[4194304]{0:T(1024)(128)(4,1)S(1)}, s32[]{:S(2)}) async-start(s8[6291456]{0:T(1024)(128)(4,1)} %bitcast.34), calls=%async_computation.10 | async-start | bytes 8388608
  904.2 6.4 slice-start.1
  913.3 12.7 %slice-start.2 = ((s8[6291456]{0:T(1024)(128)(4,1)}), s8[4194304]{0:T(1024)(128)(4,1)S(1)}, s32[]{:S(2)}) async-start(s8[6291456]{0:T(1024)(128)(4,1)} %bitcast.36), calls=%async_computation.12 | async-start | bytes 8388608
  919.6 6.4 slice-start.3
Sparse Core Ops, SparseCore 0:
  13.6 49.0 all-gather.6
  64.9 46.3 all-gather.8
  113.4 46.3 all-gather.12
  221.0 46.7 all-gather.14
  363.8 46.7 all-gather.10
  506.1 46.7 all-gather.16
